TPU v7x, 32 devices: a whole 2x2x4 slice. The times are simulated.
32 devices in a mesh: sp: 4 (over z), dp: 8 (over y, x, core).
Axes of the slice: x: 2, y: 2, z: 4, core: 2. Of those that a mesh axis runs over, the one named last changes fastest.
Arguments:
- hidden_states: bfloat16 [8, 512, 2048], P('dp', 'sp'), may hold values from -6 to 6
- queries: bfloat16 [8, 512, 2048], P('dp', 'sp'), may hold values from -12 to 12
- key_shift: bfloat16 [8, 512, 16], P('dp', 'sp'), may hold values from -15 to 0
- key_weight: bfloat16 [2048, 256], P('dp'), may hold values from -0.125 to 0.125
- value_weight: bfloat16 [2048, 256], P('dp'), may hold values from -0.125 to 0.125
Outputs:
- attended: bfloat16 [8, 512, 2048], P('dp', 'sp')
All inputs are finite; a program needn't handle non-finite values.
Results may differ from a plain program's by a relative error of at most 0.0079.
Values may be sent and summed in bfloat16 or wider, within the bound.
A program may use at most 64 MiB of HBM per device.

v0:
```python
import jax
import jax.numpy as jnp
from jax import lax
from jax.sharding import PartitionSpec as P

QUERY_HEAD_COUNT = 16
HEAD_DIM = 128


def attend(queries, key_all, value_all, shift_all):
    length, head_count, head_dim = queries.shape
    block_len = min(512, length)
    block_count = length // block_len
    scaling = head_dim ** (-0.5)
    shift_float = shift_all.astype(jnp.float32)
    offsets = jnp.arange(block_len, dtype=jnp.int32)

    def over_queries(block_index, outputs):
        first_row = block_index * block_len
        query_tile = lax.dynamic_slice_in_dim(queries, first_row, block_len, 0)

        def over_keys(back_step, state_pair):
            running, carried = state_pair
            key_start = (block_index - back_step) * block_len
            key_tile = lax.dynamic_slice_in_dim(key_all, key_start, block_len, 0)
            value_tile = lax.dynamic_slice_in_dim(value_all, key_start, block_len, 0)
            shift_tile = lax.dynamic_slice_in_dim(shift_float, key_start, block_len, 0)
            logits = jnp.einsum(
                "qhd,khd->hqk", query_tile, key_tile, preferred_element_type=jnp.float32
            )
            logits = logits * scaling + shift_tile.T[:, None, :]
            visible = (key_start + offsets)[None, :] < (first_row + offsets)[:, None]
            penalty = jnp.where(visible, jax.nn.softplus(logits), 0.0)
            suffix_sum = lax.cumsum(penalty, axis=2, reverse=True) - penalty + carried[:, :, None]
            weights = jnp.where(
                visible, jnp.exp(jax.nn.log_sigmoid(logits) - suffix_sum), 0.0
            ).astype(jnp.bfloat16)
            running = running + jnp.einsum(
                "hqk,khd->hqd", weights, value_tile, preferred_element_type=jnp.float32
            )
            return (running, carried + jnp.sum(penalty, axis=2))

        initial = (
            jnp.zeros((head_count, block_len, head_dim), jnp.float32),
            jnp.zeros((head_count, block_len), jnp.float32),
        )
        running, carried = lax.fori_loop(0, block_index + 1, over_keys, initial)
        finished = jnp.transpose(running, (1, 0, 2)).astype(jnp.bfloat16)
        return lax.dynamic_update_slice_in_dim(outputs, finished, first_row, 0)

    return lax.fori_loop(0, block_count, over_queries, jnp.zeros(queries.shape, jnp.bfloat16))


def per_device(hidden_states, queries, key_shift, key_weight, value_weight):
    seq_local, tok_local, model_dim = hidden_states.shape
    token_rows = hidden_states.reshape(seq_local * tok_local, model_dim)
    key_sum = jnp.dot(
        token_rows,
        lax.all_gather(key_weight, "dp", axis=0, tiled=True),
        preferred_element_type=jnp.float32,
    )
    value_sum = jnp.dot(
        token_rows,
        lax.all_gather(value_weight, "dp", axis=0, tiled=True),
        preferred_element_type=jnp.float32,
    )
    shared_heads = key_weight.shape[1] // HEAD_DIM
    key_local = key_sum.astype(jnp.bfloat16).reshape(seq_local, tok_local, shared_heads, HEAD_DIM)
    value_local = value_sum.astype(jnp.bfloat16).reshape(
        seq_local, tok_local, shared_heads, HEAD_DIM
    )
    query_local = queries.reshape(seq_local, tok_local, QUERY_HEAD_COUNT, HEAD_DIM)
    group_size = QUERY_HEAD_COUNT // shared_heads
    key_wide = jnp.repeat(key_local, group_size, axis=2)
    value_wide = jnp.repeat(value_local, group_size, axis=2)
    query_heads, key_heads, value_heads, shift_heads = (
        lax.all_to_all(query_local, "sp", split_axis=2, concat_axis=1, tiled=True),
        lax.all_to_all(key_wide, "sp", split_axis=2, concat_axis=1, tiled=True),
        lax.all_to_all(value_wide, "sp", split_axis=2, concat_axis=1, tiled=True),
        lax.all_to_all(key_shift, "sp", split_axis=2, concat_axis=1, tiled=True),
    )
    outputs = jax.vmap(attend)(query_heads, key_heads, value_heads, shift_heads)
    returned = lax.all_to_all(outputs, "sp", split_axis=1, concat_axis=2, tiled=True)
    return returned.reshape(seq_local, tok_local, QUERY_HEAD_COUNT * HEAD_DIM)


def solution(mesh):
    placed = (
        P("dp", "sp", None),
        P("dp", "sp", None),
        P("dp", "sp", None),
        P("dp", None),
        P("dp", None),
    )
    return jax.shard_map(
        per_device, mesh=mesh, in_specs=placed, out_specs=P("dp", "sp", None), check_vma=False
    )
```

profile of v0, /device:TPU:0, one launch (start us, length us, event | category | flops | bytes accessed | tf_op | source)
XLA Modules:
  0.0 132.7 jit_solution(17721567945287426333)
XLA Ops:
  6.5 0.7 all-gather.3.cloned.1.call-update
  7.3 0.0 all-gather.5.cloned.1.call-start
  7.3 0.7 all-gather.5.cloned.1.call-update
  8.0 0.7 copy.54
  8.7 0.5 broadcast.134
  9.2 0.7 reduce.9
  9.9 0.6 reshape.251
  10.5 6.3 %all-to-all-start.2 = ((bf16[4,2,256]{2,1,0:T(2,128)(2,1)}), bf16[4,2,256]{2,1,0:T(2,128)(2,1)S(1)}, u32[]{:S(2)}, u32[]{:S(2)}) async-start(bf16[4,2,256]{2,1,0:T(2,128)(2,1)} %reshape.251), calls=%async_computation.2 | async-start | bytes 8192 | tf_op jit(solution)/shard_map/all_to_all | solution.py:80
  16.8 2.0 %copy.32 = bf16[1,128,2048]{1,2,0:T(8,128)(2,1)} copy(bf16[1,128,2048]{2,1,0:T(8,128)(2,1)} %param.8) | data formatting | bytes 1048576 | tf_op args[1]
  18.9 3.4 %all-to-all-done.2 = bf16[4,2,256]{2,1,0:T(2,128)(2,1)S(1)} async-done(((bf16[4,2,256]{2,1,0:T(2,128)(2,1)}), bf16[4,2,256]{2,1,0:T(2,128)(2,1)S(1)}, u32[]{:S(2)}, u32[]{:S(2)}) %all-to-all-start.2) | async-done | bytes 4128 | tf_op jit(solution)/shard_map/all_to_all | solution.py:80
  22.3 3.5 %all-to-all-start = ((bf16[1,128,16,128]{1,3,0,2:T(8,128)(2,1)}), bf16[1,128,16,128]{1,3,0,2:T(8,128)(2,1)S(1)}, u32[]{:S(2)}, u32[]{:S(2)}) async-start(bf16[1,128,16,128]{1,3,0,2:T(8,128)(2,1)} %bitcast.6), calls=%async_computation | async-start | bytes 1048576 | tf_op jit(solution)/shard_map/all_to_all | solution.py:77
  25.8 9.6 %all-gather.3.cloned.1.call-done = bf16[2048,256]{1,0:T(8,128)(2,1)} async-done(((bf16[256,256]{1,0:T(8,128)(2,1)}), bf16[2048,256]{1,0:T(8,128)(2,1)}) %all-gather.3.cloned.1.call-update) | async-done | bytes 1048592 | tf_op jit(solution)/shard_map/all_gather | solution.py:59
  35.4 1.5 %fusion.14 = bf16[16,2,8,128]{3,2,1,0:T(8,128)(2,1)S(1)} fusion(bf16[2048,256]{1,0:T(8,128)(2,1)} %all-gather.3.cloned.1.call-done, bf16[1,128,2048]{2,1,0:T(8,128)(2,1)S(1)} %copy-done), kind=kOutput, calls=%fused_computation.24 | convolution fusion | flops 134250496 | bytes 1638400 | tf_op jit(solution)/shard_map/dot_general | solution.py:57
  36.9 2.3 %all-to-all-done = bf16[1,128,16,128]{1,3,0,2:T(8,128)(2,1)S(1)} async-done(((bf16[1,128,16,128]{1,3,0,2:T(8,128)(2,1)}), bf16[1,128,16,128]{1,3,0,2:T(8,128)(2,1)S(1)}, u32[]{:S(2)}, u32[]{:S(2)}) %all-to-all-start) | async-done | bytes 524320 | tf_op jit(solution)/shard_map/all_to_all | solution.py:77
  39.2 0.9 broadcast_in_dim.36
  40.1 3.5 %all-to-all-start.1 = ((bf16[1,128,16,128]{3,1,0,2:T(8,128)(2,1)}), bf16[1,128,16,128]{3,1,0,2:T(8,128)(2,1)S(1)}, u32[]{:S(2)}, u32[]{:S(2)}) async-start(bf16[1,128,16,128]{3,1,0,2:T(8,128)(2,1)} %bitcast.1), calls=%async_computation.1 | async-start | bytes 1048576 | tf_op jit(solution)/shard_map/all_to_all | solution.py:78
  43.6 0.1 iota_compare_fusion
  43.7 0.3 copy.34
  44.0 16.6 %all-gather.5.cloned.1.call-done = bf16[2048,256]{1,0:T(8,128)(2,1)} async-done(((bf16[256,256]{1,0:T(8,128)(2,1)}), bf16[2048,256]{1,0:T(8,128)(2,1)}) %all-gather.5.cloned.1.call-update) | async-done | bytes 1048592 | tf_op jit(solution)/shard_map/all_gather | solution.py:64
  60.6 1.5 %fusion.15 = bf16[16,2,8,128]{3,2,1,0:T(8,128)(2,1)S(1)} fusion(bf16[2048,256]{1,0:T(8,128)(2,1)} %all-gather.5.cloned.1.call-done, bf16[1,128,2048]{2,1,0:T(8,128)(2,1)S(1)} %copy-done), kind=kOutput, calls=%fused_computation.25 | convolution fusion | flops 134250496 | bytes 1638400 | tf_op jit(solution)/shard_map/dot_general | solution.py:62
  62.2 0.9 broadcast_in_dim.38
  63.1 4.6 %all-to-all-start.3 = ((bf16[1,128,16,128]{3,1,0,2:T(8,128)(2,1)}), bf16[1,128,16,128]{3,1,0,2:T(8,128)(2,1)S(1)}, u32[]{:S(2)}, u32[]{:S(2)}) async-start(bf16[1,128,16,128]{3,1,0,2:T(8,128)(2,1)} %bitcast.21), calls=%async_computation.3 | async-start | bytes 1048576 | tf_op jit(solution)/shard_map/all_to_all | solution.py:79
  67.7 4.4 %fusion.5 = (f32[4,512,512]{1,2,0:T(8,128)S(1)}, f32[4,512,512]{2,1,0:T(8,128)}) fusion(f32[4,512]{1,0:T(4,128)S(1)} %bitcast.103, pred[512,512]{0,1:T(8,128)(4,1)S(1)} %iota_compare_fusion, bf16[512,4,128]{2,0,1:T(8,128)(2,1)S(1)} %bitcast.100, bf16[512,4,128]{2,0,1:T(8,128)(2,1)S(1)} %bitcast.99), kind=kOutput, calls=%fused_computation.7 | convolution fusion | flops 277872640 | bytes 9707520 | tf_op jit(solution)/shard_map/vmap()/while/body/eval_jaxpr/while/body/qhd,khd->hqk/dot_general | solution.py:28
  72.2 19.6 %fusion.11 = f32[1,4,512,4,128]{2,3,4,1,0:T(4,128)S(1)} fusion(f32[1,4,512,4,128]{2,4,3,1,0:T(8,128)S(1)} %bitcast.93), kind=kOutput, calls=%fused_computation.17 | output fusion | flops 133169152 | bytes 8388608 | tf_op jit(solution)/shard_map/reduce-window.8
  91.8 3.3 %copy.38 = f32[1,4,512,4,128]{2,4,3,1,0:T(8,128)} copy(f32[1,4,512,4,128]{2,3,4,1,0:T(4,128)S(1)} %fusion.11) | data formatting | bytes 8388608 | tf_op jit(solution)/shard_map/reduce-window.8
  95.0 0.1 reduce-window.19
  95.2 8.8 %fusion.4 = bf16[4,512,512]{1,2,0:T(8,128)(2,1)S(1)} fusion(f32[4,512,512]{1,2,0:T(8,128)} %bitcast.92, f32[4,512,512]{2,1,0:T(8,128)} %get-tuple-element.133, f32[4,512]{1,0:T(4,128)S(1)} %bitcast.104, f32[4,512,4]{1,2,0:T(4,128)S(1)} %slice_bitcast_fusion, pred[512,512]{0,1:T(8,128)(4,1)S(1)} %iota_compare_fusion), kind=kLoop, calls=%fused_computation.6 | loop fusion | flops 23068672 | bytes 10788864 | tf_op jit(solution)/shard_map/vmap()/while/body/eval_jaxpr/while/body/convert_element_type | solution.py:37
  104.0 0.9 fusion.13
  104.9 0.4 copy.42
  105.3 19.2 %all_to_all.78 = bf16[1,512,4,128]{3,2,0,1:T(4,128)(2,1)S(1)} all-to-all(bf16[1,512,4,128]{3,2,0,1:T(4,128)(2,1)S(1)} %copy.42), channel_id=1, replica_groups=mesh['sp'=4,'dp'=8] {'sp'}, dimensions={1} | all-to-all | bytes 1048576 | tf_op jit(solution)/shard_map/all_to_all | solution.py:83
  124.5 0.2 copy.43
  124.7 1.2 reshape.241
  (14 shorter events, 0.2 us)
Async XLA Ops:
  6.5 28.8 %copy-start = (bf16[1,128,2048]{2,1,0:T(8,128)(2,1)S(1)}, bf16[1,128,2048]{2,1,0:T(8,128)(2,1)}, u32[]{:S(2)}) copy-start(bf16[1,128,2048]{2,1,0:T(8,128)(2,1)} %param.7) | copy-start | bytes 1572868
  6.5 28.8 %all-gather.3.cloned.1.call-start = ((), (), s32[]{:S(2)}) async-start(), calls=%async_computation.5 | async-start | bytes 1179648 | tf_op jit(solution)/shard_map/all_gather | solution.py:59
  7.3 53.4 %all-gather.5.cloned.1.call-start = ((), (), s32[]{:S(2)}) async-start(), calls=%async_computation.6 | async-start | bytes 1179648 | tf_op jit(solution)/shard_map/all_gather | solution.py:64
  10.5 11.8 %all-to-all-start.2 = ((bf16[4,2,256]{2,1,0:T(2,128)(2,1)}), bf16[4,2,256]{2,1,0:T(2,128)(2,1)S(1)}, u32[]{:S(2)}, u32[]{:S(2)}) async-start(bf16[4,2,256]{2,1,0:T(2,128)(2,1)} %reshape.251), calls=%async_computation.2 | async-start | bytes 8192 | tf_op jit(solution)/shard_map/all_to_all | solution.py:80
  22.3 16.9 %all-to-all-start = ((bf16[1,128,16,128]{1,3,0,2:T(8,128)(2,1)}), bf16[1,128,16,128]{1,3,0,2:T(8,128)(2,1)S(1)}, u32[]{:S(2)}, u32[]{:S(2)}) async-start(bf16[1,128,16,128]{1,3,0,2:T(8,128)(2,1)} %bitcast.6), calls=%async_computation | async-start | bytes 1048576 | tf_op jit(solution)/shard_map/all_to_all | solution.py:77
  40.1 22.1 %all-to-all-start.1 = ((bf16[1,128,16,128]{3,1,0,2:T(8,128)(2,1)}), bf16[1,128,16,128]{3,1,0,2:T(8,128)(2,1)S(1)}, u32[]{:S(2)}, u32[]{:S(2)}) async-start(bf16[1,128,16,128]{3,1,0,2:T(8,128)(2,1)} %bitcast.1), calls=%async_computation.1 | async-start | bytes 1048576 | tf_op jit(solution)/shard_map/all_to_all | solution.py:78
  63.1 32.0 %all-to-all-start.3 = ((bf16[1,128,16,128]{3,1,0,2:T(8,128)(2,1)}), bf16[1,128,16,128]{3,1,0,2:T(8,128)(2,1)S(1)}, u32[]{:S(2)}, u32[]{:S(2)}) async-start(bf16[1,128,16,128]{3,1,0,2:T(8,128)(2,1)} %bitcast.21), calls=%async_computation.3 | async-start | bytes 1048576 | tf_op jit(solution)/shard_map/all_to_all | solution.py:79
Sparse Core Ops, SparseCore 0:
  9.2 26.0 all-gather.2
  37.2 23.3 all-gather.4
where the time goes:
time: 133 us
  waiting for transfers between devices  33.3 us (25%)
  other arithmetic  29.2 us (22%)
  blocking collectives  19.2 us (14%)
  starting transfers between devices  17.9 us (13%)
  between operations  13.6 us (10%)
  local copies, waits for them, and re-layouts  11.1 us (8%)
  matrix products  8.43 us (6%)
    another operation x2, other arithmetic  19.6 us
    all_to_all x1, blocking collectives, per_device(): lax.all_to_all(outputs, 'sp', split_axis=1, concat_axis=2, tiled=True)  19.2 us
    all_gather x1, waiting for transfers between devices, per_device(): lax.all_gather(value_weight, 'dp', axis=0, tiled=True)  16.6 us
    all_gather x1, waiting for transfers between devices, per_device(): lax.all_gather(key_weight, 'dp', axis=0, tiled=True)  9.59 us
    convert_element_type x1, other arithmetic, over_keys(): weights = jnp.where(visible, jnp.exp(jax.nn.log_sigmoid(logits) - suffix_...  8.78 us
    all_to_all x1, starting transfers between devices, per_device(): lax.all_to_all(key_shift, 'sp', split_axis=2, concat_axis=1, tiled=True)  6.35 us
    all_to_all x1, starting transfers between devices, per_device(): lax.all_to_all(value_wide, 'sp', split_axis=2, concat_axis=1, tiled=True)  4.6 us
    dot_general x1, matrix products, over_keys(): jnp.einsum('qhd,khd->hqk', query_tile, key_tile, preferred_element_type=j...  4.44 us
  transfers between devices with their start and end apart: 6, of which 4 were waited for; matrix products, arithmetic and copies ran while one was open for 27% of the time, Pallas kernels for 0%

commit v1 on v0

v1 whole, which is shorter than its diff:
```python
import functools
import math

import jax
import jax.numpy as jnp
from jax import lax
from jax.experimental import pallas as pl
from jax.experimental.pallas import tpu as pltpu
from jax.sharding import PartitionSpec as P

HEAD_DIM = 128
LOG2E = math.log2(math.e)
MESH = pl.DeviceIdType.MESH
NT = (((1,), (1,)), ((), ()))


def chip_peers(chip, chips):
    if chips == 4:
        x, y = chip % 2, chip // 2
        order = [chip + 1 - 2 * x, chip + 2 - 4 * y, chips - 1 - chip]
        return [(c, c) for c in order]
    return [((chip + k) % chips, (chip + chips - k) % chips) for k in range(1, chips)]


def kernel(
    n_sp, n_dp,
    x_hbm, q_hbm, sh_hbm, wk_hbm, wv_hbm, out_ref,
    x, q, sh, w_all, kv, sh_all, wts, acc, carried, tri,
    load_sem, ici_send, ici_recv, d2d_send, d2d_recv, z_send, z_recv,
):
    s, d = lax.axis_index("sp"), lax.axis_index("dp")
    chips = n_dp // 2
    chip, core = d // 2, d % 2
    partner = d + 1 - 2 * core
    peers = chip_peers(chip, chips)
    tok, model = x.shape
    heads = sh.shape[1]
    groups = kv.shape[3] // HEAD_DIM
    per_group = heads // groups

    loads = [
        pltpu.make_async_copy(wk_hbm, w_all.at[0, d], load_sem.at[0]),
        pltpu.make_async_copy(wv_hbm, w_all.at[1, d], load_sem.at[1]),
        pltpu.make_async_copy(sh_hbm, sh, load_sem.at[2]),
        pltpu.make_async_copy(x_hbm, x, load_sem.at[3]),
        pltpu.make_async_copy(q_hbm, q, load_sem.at[4]),
    ]
    for load in loads:
        load.start()

    barrier = pltpu.get_barrier_semaphore()
    for to, _ in peers:
        pl.semaphore_signal(barrier, inc=1, device_id={"dp": to * 2 + core}, device_id_type=MESH)
    pl.semaphore_signal(barrier, inc=1, device_id={"dp": partner}, device_id_type=MESH)
    for t in range(1, n_sp):
        pl.semaphore_signal(barrier, inc=1, device_id={"sp": (s + t) % n_sp}, device_id_type=MESH)
    pl.semaphore_wait(barrier, chips - 1 + 1 + n_sp - 1)

    def ici_copy(part, k, block, to):
        return pltpu.make_async_remote_copy(
            src_ref=w_all.at[part, block], dst_ref=w_all.at[part, block],
            send_sem=ici_send.at[part, k], recv_sem=ici_recv.at[part, k],
            device_id={"dp": to * 2 + core}, device_id_type=MESH)

    def d2d_copy(part, k, block):
        return pltpu.make_async_remote_copy(
            src_ref=w_all.at[part, block], dst_ref=w_all.at[part, block],
            send_sem=d2d_send.at[part, k], recv_sem=d2d_recv.at[part, k],
            device_id={"dp": partner}, device_id_type=MESH)

    def z_copy(part, t, block, to):
        ref = sh_all.at[block] if part == 2 else kv.at[part, block]
        return pltpu.make_async_remote_copy(
            src_ref=ref, dst_ref=ref,
            send_sem=z_send.at[part, t], recv_sem=z_recv.at[part, t],
            device_id={"sp": to}, device_id_type=MESH)

    for part in range(2):
        loads[part].wait()
        for k, (to, _) in enumerate(peers, 1):
            ici_copy(part, k, d, to).start()
        d2d_copy(part, 0, d).start()

    loads[2].wait()
    eye = (
        lax.broadcasted_iota(jnp.int32, (heads, heads), 0)
        == lax.broadcasted_iota(jnp.int32, (heads, heads), 1)
    ).astype(jnp.bfloat16)
    sh_all[s] = lax.dot_general(eye, sh[...], NT, preferred_element_type=jnp.float32).astype(jnp.bfloat16)
    row = lax.broadcasted_iota(jnp.int32, tri.shape, 0)
    col = lax.broadcasted_iota(jnp.int32, tri.shape, 1)
    tri[...] = ((row > col) | (col >= tok)).astype(jnp.bfloat16)

    def send_up(part):
        for t in range(1, n_sp):
            @pl.when(s + t < n_sp)
            def _(t=t):
                z_copy(part, t, s, s + t).start()

    send_up(2)

    def gather(part):
        for k, (_, source) in enumerate(peers, 1):
            block = source * 2 + core
            ici_copy(part, k, block, chip).wait_recv()
            d2d_copy(part, k, block).start()
        d2d_copy(part, 0, partner).wait_recv()
        for k, (_, source) in enumerate(peers, 1):
            d2d_copy(part, k, source * 2 + 1 - core).wait_recv()

    def project(part):
        weight = w_all[part].reshape(model, w_all.shape[3])
        kv[part, s] = jnp.dot(x[...], weight, preferred_element_type=jnp.float32).astype(jnp.bfloat16)

    def weigh(block, diagonal):
        keys = kv[0, block]
        shift = sh_all[block].astype(jnp.float32) * LOG2E
        scale = HEAD_DIM ** -0.5 * LOG2E
        if diagonal:
            visible = lax.broadcasted_iota(jnp.int32, (tok, tok), 1) < lax.broadcasted_iota(
                jnp.int32, (tok, tok), 0)
        for h in range(heads):
            g = h // per_group
            z = lax.dot_general(
                q[:, h * HEAD_DIM:(h + 1) * HEAD_DIM], keys[:, g * HEAD_DIM:(g + 1) * HEAD_DIM], NT,
                preferred_element_type=jnp.float32)
            z = z * scale + shift[h:h + 1, :]
            p = jnp.maximum(z, jnp.log(1.0 + jnp.exp2(jnp.minimum(z, 100.0))) * LOG2E)
            if diagonal:
                p = jnp.where(visible, p, 0.0)
            sums = jnp.dot(p.astype(jnp.bfloat16), tri[...], preferred_element_type=jnp.float32)
            power = z - p - sums[:, :tok]
            total = sums[:, tok:]
            if diagonal:
                w = jnp.where(visible, jnp.exp2(power), 0.0)
                carried[h] = total
            else:
                before = carried[h]
                w = jnp.exp2(power - before)
                carried[h] = before + total
            wts[block, h] = w.astype(jnp.bfloat16)

    def mix(block, first):
        values = kv[1, block]
        for g in range(groups):
            span = slice(g * per_group, (g + 1) * per_group)
            w = wts[block, span].reshape(per_group * tok, tok)
            term = jnp.dot(w, values[:, g * HEAD_DIM:(g + 1) * HEAD_DIM], preferred_element_type=jnp.float32)
            term = term.reshape(per_group, tok, HEAD_DIM)
            acc[span] = term if first else acc[span] + term

    gather(0)
    loads[3].wait()
    project(0)
    send_up(0)
    loads[4].wait()
    weigh(s, True)
    gather(1)
    project(1)
    send_up(1)

    @pl.loop(1, s + 1)
    def _(t):
        z_copy(2, t, s - t, s).wait_recv()
        z_copy(0, t, s - t, s).wait_recv()
        weigh(s - t, False)

    mix(s, True)

    @pl.loop(1, s + 1)
    def _(t):
        z_copy(1, t, s - t, s).wait_recv()
        mix(s - t, False)

    for h in range(heads):
        out_ref[:, h * HEAD_DIM:(h + 1) * HEAD_DIM] = acc[h].astype(out_ref.dtype)

    for part in range(2):
        for k, (to, source) in enumerate(peers, 1):
            ici_copy(part, k, d, to).wait_send()
            d2d_copy(part, k, source * 2 + core).wait_send()
        d2d_copy(part, 0, d).wait_send()
    for part in range(3):
        for t in range(1, n_sp):
            @pl.when(s + t < n_sp)
            def _(part=part, t=t):
                z_copy(part, t, s, s + t).wait_send()


def per_device(n_sp, n_dp, hidden_states, queries, key_shift, key_weight, value_weight):
    seq_local, tok, model = hidden_states.shape
    assert seq_local == 1
    width, heads = queries.shape[2], key_shift.shape[2]
    rows, kv_width = key_weight.shape
    chips = n_dp // 2
    bf16, f32 = jnp.bfloat16, jnp.float32
    dma = pltpu.SemaphoreType.DMA
    out = pl.pallas_call(
        functools.partial(kernel, n_sp, n_dp),
        out_shape=jax.ShapeDtypeStruct((tok, width), bf16),
        in_specs=[pl.BlockSpec(memory_space=pl.ANY)] * 5,
        out_specs=pl.BlockSpec(memory_space=pltpu.VMEM),
        scratch_shapes=[
            pltpu.VMEM((tok, model), bf16),
            pltpu.VMEM((tok, width), bf16),
            pltpu.VMEM((tok, heads), bf16),
            pltpu.VMEM((2, n_dp, rows, kv_width), bf16),
            pltpu.VMEM((2, n_sp, tok, kv_width), bf16),
            pltpu.VMEM((n_sp, heads, tok), bf16),
            pltpu.VMEM((n_sp, heads, tok, tok), bf16),
            pltpu.VMEM((heads, tok, HEAD_DIM), f32),
            pltpu.VMEM((heads, tok, tok), f32),
            pltpu.VMEM((tok, 2 * tok), bf16),
            dma((5,)),
            dma((2, chips)), dma((2, chips)),
            dma((2, chips)), dma((2, chips)),
            dma((3, n_sp)), dma((3, n_sp)),
        ],
        compiler_params=pltpu.CompilerParams(collective_id=0, has_side_effects=True),
        name="stick_breaking",
    )(hidden_states[0], queries[0], key_shift[0], key_weight, value_weight)
    return out[None]


def solution(mesh):
    placed = (
        P("dp", "sp", None),
        P("dp", "sp", None),
        P("dp", "sp", None),
        P("dp", None),
        P("dp", None),
    )
    return jax.shard_map(
        functools.partial(per_device, mesh.shape["sp"], mesh.shape["dp"]),
        mesh=mesh, in_specs=placed, out_specs=P("dp", "sp", None), check_vma=False,
    )
```

time: 133 us -> 32.3 us (0.24)
  the two profiles are of different devices: /device:TPU:0 before, /device:TPU:25 now
where the time goes in v1:
time: 32.3 us; the launch traced here: 32.1 us
  Pallas kernels  28.8 us (89%)
  local copies, waits for them, and re-layouts  3.28 us (10%)
    pallas_call x1, Pallas kernels, per_device(): pl.pallas_call(functools.partial(kernel, n_sp, n_dp), out_shape=jax.Shape...  28.8 us
    unnamed x2, local copies, waits for them, and re-layouts  3.28 us

profile of v1, /device:TPU:25, one launch (start us, length us, event | category | flops | bytes accessed | tf_op | source)
XLA Modules:
  0.0 32.1 jit_solution(13643237426803230201)
XLA Ops:
  0.0 1.4 %copy.6 = bf16[1,128,16]{2,1,0:T(8,128)(2,1)} copy(bf16[1,128,16]{1,2,0:T(8,128)(2,1)} %param.7) | data formatting | bytes 8192 | tf_op args[2]
  1.4 28.8 %stick_breaking.1 = bf16[128,2048]{1,0:T(8,128)(2,1)} custom-call(bf16[128,2048]{1,0:T(8,128)(2,1)} %bitcast.5, bf16[128,2048]{1,0:T(8,128)(2,1)} %bitcast.6, bf16[128,16]{1,0:T(8,128)(2,1)} %bitcast.7, bf16[256,256]{1,0:T(8,128)(2,1)} %wk_hbm.1, bf16[256,256]{1,0:T(8,128)(2,1)} %wv_hbm.1), custom_call_target="tpu_custom_call" | custom-call | tf_op jit(solution)/shard_map/stick_breaking/pallas_call | solution.py:198
  30.2 1.9 %copy.8 = bf16[1,128,2048]{2,1,0:T(8,128)(2,1)} copy(bf16[1,128,2048]{2,1,0:T(8,128)(2,1)} %bitcast.4) | data formatting | bytes 1048576

commit v2 on v1

v2 whole, which is shorter than its diff:
```python
import functools
import math

import jax
import jax.numpy as jnp
from jax import lax
from jax.experimental import pallas as pl
from jax.experimental.pallas import tpu as pltpu
from jax.sharding import PartitionSpec as P

HEAD_DIM = 128
LOG2E = math.log2(math.e)
MESH = pl.DeviceIdType.MESH
NT = (((1,), (1,)), ((), ()))


def chip_peers(chip, chips):
    if chips == 4:
        x, y = chip % 2, chip // 2
        order = [chip + 1 - 2 * x, chip + 2 - 4 * y, chips - 1 - chip]
        return [(c, c) for c in order]
    return [((chip + k) % chips, (chip + chips - k) % chips) for k in range(1, chips)]


def kernel(
    n_sp, n_dp,
    x_hbm, q_hbm, sh_hbm, wk_hbm, wv_hbm, out_ref,
    x, q, w_all, kv, sh_all, wts, acc, carried, tri,
    load_sem, ici_send, ici_recv, d2d_send, d2d_recv, z_send, z_recv,
):
    s, d = lax.axis_index("sp"), lax.axis_index("dp")
    chips = n_dp // 2
    chip, core = d // 2, d % 2
    partner = d + 1 - 2 * core
    peers = chip_peers(chip, chips)
    relay = chips == 4
    tok = x.shape[0]
    heads = sh_all.shape[1]
    parts = kv.shape[0]
    groups = parts // 2
    per_group = heads // groups

    loads = []
    for part in range(parts):
        source = (wk_hbm, wv_hbm)[part // groups].at[:, pl.ds(part % groups * HEAD_DIM, HEAD_DIM)]
        loads.append(pltpu.make_async_copy(source, w_all.at[part, d], load_sem.at[part]))
    load_sh = pltpu.make_async_copy(sh_hbm, sh_all.at[s], load_sem.at[parts])
    load_x = pltpu.make_async_copy(x_hbm, x, load_sem.at[parts + 1])
    load_q = pltpu.make_async_copy(q_hbm, q, load_sem.at[parts + 2])
    for load in loads + [load_sh, load_x, load_q]:
        load.start()

    barrier = pltpu.get_barrier_semaphore()
    for to, _ in peers:
        pl.semaphore_signal(barrier, inc=1, device_id={"dp": to * 2 + core}, device_id_type=MESH)
    pl.semaphore_signal(barrier, inc=1, device_id={"dp": partner}, device_id_type=MESH)
    for t in range(1, n_sp):
        pl.semaphore_signal(barrier, inc=1, device_id={"sp": (s + t) % n_sp}, device_id_type=MESH)
    row = lax.broadcasted_iota(jnp.int32, tri.shape, 0)
    col = lax.broadcasted_iota(jnp.int32, tri.shape, 1)
    tri[...] = ((row > col) | (col >= tok)).astype(jnp.bfloat16)
    pl.semaphore_wait(barrier, chips - 1 + 1 + n_sp - 1)

    def ici_copy(part, k, block, to):
        return pltpu.make_async_remote_copy(
            src_ref=w_all.at[part, block], dst_ref=w_all.at[part, block],
            send_sem=ici_send.at[part, k], recv_sem=ici_recv.at[part, k],
            device_id={"dp": to * 2 + core}, device_id_type=MESH)

    def d2d_copy(part, k, block):
        return pltpu.make_async_remote_copy(
            src_ref=w_all.at[part, block], dst_ref=w_all.at[part, block],
            send_sem=d2d_send.at[part, k], recv_sem=d2d_recv.at[part, k],
            device_id={"dp": partner}, device_id_type=MESH)

    def z_copy(part, t, block, to):
        ref = sh_all.at[block] if part == parts else kv.at[part, block]
        return pltpu.make_async_remote_copy(
            src_ref=ref, dst_ref=ref,
            send_sem=z_send.at[part, t], recv_sem=z_recv.at[part, t],
            device_id={"sp": to}, device_id_type=MESH)

    def send_up(part):
        for t in range(1, n_sp):
            @pl.when(s + t < n_sp)
            def _(t=t):
                z_copy(part, t, s, s + t).start()

    def send_own(part):
        loads[part].wait()
        for k, (to, _) in enumerate(peers, 1):
            if not (relay and k == 3):
                ici_copy(part, k, d, to).start()
        d2d_copy(part, 0, d).start()

    def arrive(part, k):
        block = peers[k - 1][1] * 2 + core
        ici_copy(part, k, block, chip).wait_recv()
        d2d_copy(part, k, block).start()
        if relay and k < 3:
            @pl.when(core == k - 1)
            def _():
                ici_copy(part, 3, block, peers[2 - k][0]).start()

    def near(part):
        if relay:
            arrive(part, 1)
            arrive(part, 2)

    def finish(part):
        for k in range(3 if relay else 1, chips):
            arrive(part, k)
        d2d_copy(part, 0, partner).wait_recv()
        for k, (_, source) in enumerate(peers, 1):
            d2d_copy(part, k, source * 2 + 1 - core).wait_recv()
        weight = w_all[part].reshape(x.shape[1], HEAD_DIM)
        kv[part, s] = jnp.dot(x[...], weight, preferred_element_type=jnp.float32).astype(jnp.bfloat16)
        send_up(part)

    def weigh(block, diagonal):
        shift = sh_all[block].astype(jnp.float32) * LOG2E
        scale = HEAD_DIM ** -0.5 * LOG2E
        if diagonal:
            visible = lax.broadcasted_iota(jnp.int32, (tok, tok), 1) < lax.broadcasted_iota(
                jnp.int32, (tok, tok), 0)
        for h in range(heads):
            g = h // per_group
            z = lax.dot_general(
                q[:, h * HEAD_DIM:(h + 1) * HEAD_DIM], kv[g, block], NT,
                preferred_element_type=jnp.float32)
            z = z * scale + shift[h:h + 1, :]
            p = jnp.maximum(z, jnp.log(1.0 + jnp.exp2(jnp.minimum(z, 100.0))) * LOG2E)
            if diagonal:
                p = jnp.where(visible, p, 0.0)
            sums = jnp.dot(p.astype(jnp.bfloat16), tri[...], preferred_element_type=jnp.float32)
            power = z - p - sums[:, :tok]
            total = sums[:, tok:]
            if diagonal:
                w = jnp.where(visible, jnp.exp2(power), 0.0)
                carried[h] = total
            else:
                before = carried[h]
                w = jnp.exp2(power - before)
                carried[h] = before + total
            wts[block, h] = w.astype(jnp.bfloat16)

    def mix(g, block, first):
        span = slice(g * per_group, (g + 1) * per_group)
        w = wts[block, span].reshape(per_group * tok, tok)
        term = jnp.dot(w, kv[groups + g, block], preferred_element_type=jnp.float32)
        term = term.reshape(per_group, tok, HEAD_DIM)
        acc[span] = term if first else acc[span] + term

    send_own(0)
    send_own(1)
    load_sh.wait()
    send_up(parts)
    load_x.wait()
    for part in range(parts):
        near(part)
        if part + 2 < parts:
            send_own(part + 2)
        if part == parts - 1:
            load_q.wait()
            weigh(s, True)
        if part > 0:
            finish(part - 1)
    finish(parts - 1)

    @pl.loop(1, s + 1)
    def _(t):
        z_copy(parts, t, s - t, s).wait_recv()
        for g in range(groups):
            z_copy(g, t, s - t, s).wait_recv()
        weigh(s - t, False)

    for g in range(groups):
        mix(g, s, True)

    for g in range(groups):
        @pl.loop(1, s + 1)
        def _(t, g=g):
            z_copy(groups + g, t, s - t, s).wait_recv()
            mix(g, s - t, False)

    for h in range(heads):
        out_ref[:, h * HEAD_DIM:(h + 1) * HEAD_DIM] = acc[h].astype(out_ref.dtype)

    for part in range(parts):
        d2d_copy(part, 0, d).wait_send()
        for k, (to, source) in enumerate(peers, 1):
            ici_copy(part, k, d, to).wait_send()
            d2d_copy(part, k, source * 2 + core).wait_send()
    for part in range(parts + 1):
        for t in range(1, n_sp):
            @pl.when(s + t < n_sp)
            def _(part=part, t=t):
                z_copy(part, t, s, s + t).wait_send()


def per_device(n_sp, n_dp, hidden_states, queries, key_shift, key_weight, value_weight):
    seq_local, tok, model = hidden_states.shape
    assert seq_local == 1
    width, heads = queries.shape[2], key_shift.shape[2]
    rows, kv_width = key_weight.shape
    chips, parts = n_dp // 2, 2 * (kv_width // HEAD_DIM)
    bf16, f32 = jnp.bfloat16, jnp.float32
    dma = pltpu.SemaphoreType.DMA
    out = pl.pallas_call(
        functools.partial(kernel, n_sp, n_dp),
        out_shape=jax.ShapeDtypeStruct((tok, width), bf16),
        in_specs=[pl.BlockSpec(memory_space=pl.ANY)] * 5,
        out_specs=pl.BlockSpec(memory_space=pltpu.VMEM),
        scratch_shapes=[
            pltpu.VMEM((tok, model), bf16),
            pltpu.VMEM((tok, width), bf16),
            pltpu.VMEM((parts, n_dp, rows, HEAD_DIM), bf16),
            pltpu.VMEM((parts, n_sp, tok, HEAD_DIM), bf16),
            pltpu.VMEM((n_sp, heads, tok), bf16),
            pltpu.VMEM((n_sp, heads, tok, tok), bf16),
            pltpu.VMEM((heads, tok, HEAD_DIM), f32),
            pltpu.VMEM((heads, tok, tok), f32),
            pltpu.VMEM((tok, 2 * tok), bf16),
            dma((parts + 3,)),
            dma((parts, chips)), dma((parts, chips)),
            dma((parts, chips)), dma((parts, chips)),
            dma((parts + 1, n_sp)), dma((parts + 1, n_sp)),
        ],
        compiler_params=pltpu.CompilerParams(collective_id=0, has_side_effects=True),
        name="stick_breaking",
    )(hidden_states[0], queries[0], jnp.swapaxes(key_shift, 1, 2)[0], key_weight, value_weight)
    return out[None]


def solution(mesh):
    placed = (
        P("dp", "sp", None),
        P("dp", "sp", None),
        P("dp", "sp", None),
        P("dp", None),
        P("dp", None),
    )
    return jax.shard_map(
        functools.partial(per_device, mesh.shape["sp"], mesh.shape["dp"]),
        mesh=mesh, in_specs=placed, out_specs=P("dp", "sp", None), check_vma=False,
    )
```

time: 32.3 us -> 30.9 us (0.957)
  local copies, waits for them, and re-layouts: 3.28 us -> 1.88 us
    unnamed x2 -> x1, local copies, waits for them, and re-layouts: 3.28 us -> 1.88 us
where the time goes in v2:
time: 30.9 us; the launch traced here: 30.6 us
  Pallas kernels  28.7 us (93%)
  local copies, waits for them, and re-layouts  1.88 us (6%)
    pallas_call x1, Pallas kernels, per_device(): pl.pallas_call(functools.partial(kernel, n_sp, n_dp), out_shape=jax.Shape...  28.7 us
    unnamed x1, local copies, waits for them, and re-layouts  1.88 us

profile of v2, /device:TPU:25, one launch (start us, length us, event | category | flops | bytes accessed | tf_op | source)
XLA Modules:
  0.0 30.6 jit_solution(7374188530746764155)
XLA Ops:
  0.0 28.7 %stick_breaking.1 = bf16[128,2048]{1,0:T(8,128)(2,1)} custom-call(bf16[128,2048]{1,0:T(8,128)(2,1)} %bitcast.7, bf16[128,2048]{1,0:T(8,128)(2,1)} %bitcast.8, bf16[16,128]{1,0:T(8,128)(2,1)} %bitcast.9, bf16[256,256]{1,0:T(8,128)(2,1)} %wk_hbm.1, bf16[256,256]{1,0:T(8,128)(2,1)} %wv_hbm.1), custom_call_target="tpu_custom_call" | custom-call | tf_op jit(solution)/shard_map/stick_breaking/pallas_call | solution.py:209
  28.7 1.9 %copy.7 = bf16[1,128,2048]{2,1,0:T(8,128)(2,1)} copy(bf16[1,128,2048]{2,1,0:T(8,128)(2,1)} %bitcast.6) | data formatting | bytes 1048576

commit v3 on v2

--- a/solution.py
+++ b/solution.py
@@ -25,7 +25,7 @@
 def kernel(
     n_sp, n_dp,
     x_hbm, q_hbm, sh_hbm, wk_hbm, wv_hbm, out_ref,
-    x, q, w_all, kv, sh_all, wts, acc, carried, tri,
+    x, q, w_all, kv, sh_all, wts, acc, carried, tri, power, penalty,
     load_sem, ici_send, ici_recv, d2d_send, d2d_recv, z_send, z_recv,
 ):
     s, d = lax.axis_index("sp"), lax.axis_index("dp")
@@ -123,26 +123,32 @@
         if diagonal:
             visible = lax.broadcasted_iota(jnp.int32, (tok, tok), 1) < lax.broadcasted_iota(
                 jnp.int32, (tok, tok), 0)
-        for h in range(heads):
-            g = h // per_group
+        def first_pass(h, g):
             z = lax.dot_general(
-                q[:, h * HEAD_DIM:(h + 1) * HEAD_DIM], kv[g, block], NT,
-                preferred_element_type=jnp.float32)
+                q[:, h * HEAD_DIM:(h + 1) * HEAD_DIM], kv[g, block], NT, preferred_element_type=jnp.float32)
             z = z * scale + shift[h:h + 1, :]
             p = jnp.maximum(z, jnp.log(1.0 + jnp.exp2(jnp.minimum(z, 100.0))) * LOG2E)
             if diagonal:
                 p = jnp.where(visible, p, 0.0)
-            sums = jnp.dot(p.astype(jnp.bfloat16), tri[...], preferred_element_type=jnp.float32)
-            power = z - p - sums[:, :tok]
-            total = sums[:, tok:]
+            power[h] = z - p
+            penalty[h] = p.astype(jnp.bfloat16)
+
+        def second_pass(h):
+            sums = jnp.dot(penalty[h], tri[...], preferred_element_type=jnp.float32)
+            left = power[h] - sums[:, :tok]
             if diagonal:
-                w = jnp.where(visible, jnp.exp2(power), 0.0)
-                carried[h] = total
+                w = jnp.where(visible, jnp.exp2(left), 0.0)
+                carried[h] = sums[:, tok:]
             else:
                 before = carried[h]
-                w = jnp.exp2(power - before)
-                carried[h] = before + total
+                w = jnp.exp2(left - before)
+                carried[h] = before + sums[:, tok:]
             wts[block, h] = w.astype(jnp.bfloat16)
+
+        for h in range(heads):
+            first_pass(h, h // per_group)
+        for h in range(heads):
+            second_pass(h)
 
     def mix(g, block, first):
         span = slice(g * per_group, (g + 1) * per_group)
@@ -221,12 +227,15 @@
             pltpu.VMEM((heads, tok, HEAD_DIM), f32),
             pltpu.VMEM((heads, tok, tok), f32),
             pltpu.VMEM((tok, 2 * tok), bf16),
+            pltpu.VMEM((heads, tok, tok), f32),
+            pltpu.VMEM((heads, tok, tok), bf16),
             dma((parts + 3,)),
             dma((parts, chips)), dma((parts, chips)),
             dma((parts, chips)), dma((parts, chips)),
             dma((parts + 1, n_sp)), dma((parts + 1, n_sp)),
         ],
-        compiler_params=pltpu.CompilerParams(collective_id=0, has_side_effects=True),
+        compiler_params=pltpu.CompilerParams(
+            collective_id=0, has_side_effects=True),
         name="stick_breaking",
     )(hidden_states[0], queries[0], jnp.swapaxes(key_shift, 1, 2)[0], key_weight, value_weight)
     return out[None]

time: 30.9 us -> 28.7 us (0.929)
  Pallas kernels: 28.7 us -> 26.6 us
    pallas_call x1, Pallas kernels: 28.7 us -> 26.6 us  [per_device(): pl.pallas_call(functools.partial(kernel, n_sp, n_dp), out_shape=jax.Shape...]
where the time goes in v3:
time: 28.7 us; the launch traced here: 28.5 us
  Pallas kernels  26.6 us (93%)
  local copies, waits for them, and re-layouts  1.88 us (7%)
    pallas_call x1, Pallas kernels, per_device(): pl.pallas_call(functools.partial(kernel, n_sp, n_dp), out_shape=jax.Shape...  26.6 us
    unnamed x1, local copies, waits for them, and re-layouts  1.88 us

profile of v3, /device:TPU:25, one launch (start us, length us, event | category | flops | bytes accessed | tf_op | source)
XLA Modules:
  0.0 28.5 jit_solution(695508446007607175)
XLA Ops:
  0.0 26.6 %stick_breaking.1 = bf16[128,2048]{1,0:T(8,128)(2,1)} custom-call(bf16[128,2048]{1,0:T(8,128)(2,1)} %bitcast.7, bf16[128,2048]{1,0:T(8,128)(2,1)} %bitcast.8, bf16[16,128]{1,0:T(8,128)(2,1)} %bitcast.9, bf16[256,256]{1,0:T(8,128)(2,1)} %wk_hbm.1, bf16[256,256]{1,0:T(8,128)(2,1)} %wv_hbm.1), custom_call_target="tpu_custom_call" | custom-call | tf_op jit(solution)/shard_map/stick_breaking/pallas_call | solution.py:215
  26.6 1.9 %copy.7 = bf16[1,128,2048]{2,1,0:T(8,128)(2,1)} copy(bf16[1,128,2048]{2,1,0:T(8,128)(2,1)} %bitcast.6) | data formatting | bytes 1048576

commit v4 on v3

--- a/solution.py
+++ b/solution.py
@@ -24,9 +24,9 @@
 
 def kernel(
     n_sp, n_dp,
-    x_hbm, q_hbm, sh_hbm, wk_hbm, wv_hbm, out_ref,
-    x, q, w_all, kv, sh_all, wts, acc, carried, tri, power, penalty,
-    load_sem, ici_send, ici_recv, d2d_send, d2d_recv, z_send, z_recv,
+    x_hbm, q_hbm, sh_hbm, wk_hbm, wv_hbm, out_hbm,
+    x, q, w_all, kv, sh_all, wts, acc, carried, tri, power, penalty, staged,
+    load_sem, ici_send, ici_recv, d2d_send, d2d_recv, z_send, z_recv, out_sem,
 ):
     s, d = lax.axis_index("sp"), lax.axis_index("dp")
     chips = n_dp // 2
@@ -81,7 +81,7 @@
             device_id={"sp": to}, device_id_type=MESH)
 
     def send_up(part):
-        for t in range(1, n_sp):
+        for t in reversed(range(1, n_sp)):
             @pl.when(s + t < n_sp)
             def _(t=t):
                 z_copy(part, t, s, s + t).start()
@@ -183,14 +183,19 @@
     for g in range(groups):
         mix(g, s, True)
 
+    def store(g):
+        columns = pl.ds(g * per_group * HEAD_DIM, per_group * HEAD_DIM)
+        return pltpu.make_async_copy(staged.at[:, columns], out_hbm.at[:, columns], out_sem.at[g])
+
     for g in range(groups):
         @pl.loop(1, s + 1)
         def _(t, g=g):
             z_copy(groups + g, t, s - t, s).wait_recv()
             mix(g, s - t, False)
 
-    for h in range(heads):
-        out_ref[:, h * HEAD_DIM:(h + 1) * HEAD_DIM] = acc[h].astype(out_ref.dtype)
+        for h in range(g * per_group, (g + 1) * per_group):
+            staged[:, h * HEAD_DIM:(h + 1) * HEAD_DIM] = acc[h].astype(staged.dtype)
+        store(g).start()
 
     for part in range(parts):
         d2d_copy(part, 0, d).wait_send()
@@ -202,6 +207,8 @@
             @pl.when(s + t < n_sp)
             def _(part=part, t=t):
                 z_copy(part, t, s, s + t).wait_send()
+    for g in range(groups):
+        store(g).wait()
 
 
 def per_device(n_sp, n_dp, hidden_states, queries, key_shift, key_weight, value_weight):
@@ -216,7 +223,7 @@
         functools.partial(kernel, n_sp, n_dp),
         out_shape=jax.ShapeDtypeStruct((tok, width), bf16),
         in_specs=[pl.BlockSpec(memory_space=pl.ANY)] * 5,
-        out_specs=pl.BlockSpec(memory_space=pltpu.VMEM),
+        out_specs=pl.BlockSpec(memory_space=pl.ANY),
         scratch_shapes=[
             pltpu.VMEM((tok, model), bf16),
             pltpu.VMEM((tok, width), bf16),
@@ -229,10 +236,12 @@
             pltpu.VMEM((tok, 2 * tok), bf16),
             pltpu.VMEM((heads, tok, tok), f32),
             pltpu.VMEM((heads, tok, tok), bf16),
+            pltpu.VMEM((tok, width), bf16),
             dma((parts + 3,)),
             dma((parts, chips)), dma((parts, chips)),
             dma((parts, chips)), dma((parts, chips)),
             dma((parts + 1, n_sp)), dma((parts + 1, n_sp)),
+            dma((parts // 2,)),
         ],
         compiler_params=pltpu.CompilerParams(
             collective_id=0, has_side_effects=True),

time: 28.7 us -> 28.4 us (0.990)
  the two profiles are of different devices: /device:TPU:25 before, /device:TPU:17 now
where the time goes in v4:
time: 28.4 us; the launch traced here: 28.3 us
  Pallas kernels  26.4 us (93%)
  local copies, waits for them, and re-layouts  1.88 us (7%)
    pallas_call x1, Pallas kernels, per_device(): pl.pallas_call(functools.partial(kernel, n_sp, n_dp), out_shape=jax.Shape...  26.4 us
    unnamed x1, local copies, waits for them, and re-layouts  1.88 us

profile of v4, /device:TPU:17, one launch (start us, length us, event | category | flops | bytes accessed | tf_op | source)
XLA Modules:
  0.0 28.3 jit_solution(5367130211675898413)
XLA Ops:
  0.0 26.4 %stick_breaking.1 = bf16[128,2048]{1,0:T(8,128)(2,1)} custom-call(bf16[128,2048]{1,0:T(8,128)(2,1)} %bitcast.7, bf16[128,2048]{1,0:T(8,128)(2,1)} %bitcast.8, bf16[16,128]{1,0:T(8,128)(2,1)} %bitcast.9, bf16[256,256]{1,0:T(8,128)(2,1)} %wk_hbm.1, bf16[256,256]{1,0:T(8,128)(2,1)} %wv_hbm.1), custom_call_target="tpu_custom_call" | custom-call | tf_op jit(solution)/shard_map/stick_breaking/pallas_call | solution.py:222
  26.4 1.9 %copy.7 = bf16[1,128,2048]{2,1,0:T(8,128)(2,1)} copy(bf16[1,128,2048]{2,1,0:T(8,128)(2,1)} %bitcast.6) | data formatting | bytes 1048576
